TPU v7x, 32 devices: a whole 2x2x4 slice. The times are simulated.
32 devices in a mesh: sp: 16 (over z, y, core), tp: 2 (over x).
Axes of the slice: x: 2, y: 2, z: 4, core: 2. Of those that a mesh axis runs over, the one named last changes fastest.
Arguments:
- inputs: bfloat16 [2, 2048, 1024], P(None, 'sp'), may hold values from -6 to 6
- queries: bfloat16 [2, 2048, 4, 128], P(None, 'sp', 'tp'), may hold values from -6 to 6
- values: bfloat16 [2, 2048, 4, 256], P(None, 'sp', 'tp'), may hold values from -6 to 6
- out_grad: bfloat16 [2, 2048, 4, 256], P(None, 'sp', 'tp'), may hold values from -6 to 6
- key_weight: bfloat16 [1024, 4, 128], P(None, 'tp'), may hold values from -6 to 6
- decay_ahead: float32 [4], P('tp'), may hold values from -2.9 to 2.2
- decay_behind: float32 [4], P('tp'), may hold values from -2.9 to 2.2
Outputs:
- query_grad: bfloat16 [2, 2048, 4, 128], P(None, 'sp', 'tp')
- value_grad: bfloat16 [2, 2048, 4, 256], P(None, 'sp', 'tp')
- input_grad: bfloat16 [2, 2048, 1024], P('tp', 'sp')
- weight_grad: float32 [1024, 4, 128], P('sp', 'tp')
- decay_grad: float32 [2, 4], P(None, 'tp')
All inputs are finite; a program needn't handle non-finite values.
Results may differ from a plain program's by a relative error of at most 0.015.
Values may be sent and summed in bfloat16 or wider, within the bound.
A program may use at most 256 MiB of HBM per device.

v0:
```python
import math
import jax
import jax.numpy as jnp
from jax import lax
from jax.sharding import PartitionSpec as P

HIGHEST = lax.Precision.HIGHEST


def prefix(value, axis, join, neutral, backward):
    count, mine = (lax.axis_size(axis), lax.axis_index(axis))
    pieces = jax.tree.map(lambda part: lax.all_gather(part, axis), value)
    if backward:
        pieces = jax.tree.map(lambda part: part[::-1], pieces)
        mine = count - 1 - mine
    subtotal = jax.tree.map(
        lambda part, zero: jnp.full_like(part, 0) + jnp.asarray(zero, part.dtype), value, neutral
    )

    def step(position, subtotal):
        longer = join(subtotal, jax.tree.map(lambda part: part[position], pieces))
        return jax.tree.map(lambda new, old: jnp.where(position < mine, new, old), longer, subtotal)

    return lax.fori_loop(0, count - 1, step, subtotal)


def own_rows(contribution, rows, axis):
    whole = contribution(jnp.int32(0), rows * lax.axis_size(axis))
    return lax.psum_scatter(whole, axis, scatter_dimension=0, tiled=True)


def summed_rows(product, rows, axis):
    everything = product(jnp.int32(0), lax.axis_size(axis) * rows)
    own = lax.psum_scatter(everything.astype(jnp.bfloat16), axis, scatter_dimension=0, tiled=True)
    return own.astype(jnp.float32)


def link_states(earlier, later):
    return (
        earlier[0] * later[0],
        later[0] * earlier[1] + later[1],
        earlier[2] * later[2],
        later[2] * earlier[3] + later[3],
    )


def shards(inputs, queries, values, out_grad, key_weight, decay_ahead, decay_behind):
    batch_seqs, length, in_width = inputs.shape
    devices = lax.axis_size("sp")
    my_index = lax.axis_index("sp").astype(jnp.float32)
    all_tokens = length * devices
    key_scale = 1.0 / math.sqrt(in_width * queries.shape[3] * all_tokens)
    rate_ahead = jax.nn.log_sigmoid(decay_ahead) / all_tokens
    rate_behind = jax.nn.log_sigmoid(decay_behind) / all_tokens
    key_raw = jnp.einsum(
        "bld,dhk->blhk", inputs, key_weight, preferred_element_type=jnp.float32
    ).astype(jnp.bfloat16)
    keys = key_raw.astype(jnp.float32) * key_scale
    query_wide = queries.astype(jnp.float32)
    value_wide = values.astype(jnp.float32)
    grad_wide = out_grad.astype(jnp.float32)
    offsets = jnp.arange(length, dtype=jnp.float32)
    distance = offsets[:, None] - offsets[None, :]
    mask_ahead = jnp.where(
        distance[None] >= 0, jnp.exp(distance[None] * rate_ahead[:, None, None]), 0.0
    )
    mask_behind = jnp.where(
        distance[None] <= 0, jnp.exp(-distance[None] * rate_behind[:, None, None]), 0.0
    )
    mask_both = (mask_ahead + mask_behind)[None]
    keep_ahead = jnp.exp((length - 1.0 - offsets)[:, None] * rate_ahead[None])[None, :, :, None]
    keep_behind = jnp.exp(offsets[:, None] * rate_behind[None])[None, :, :, None]
    reach_ahead = jnp.exp((offsets + 1.0)[:, None] * rate_ahead[None])[None, :, :, None]
    reach_behind = jnp.exp((length - offsets)[:, None] * rate_behind[None])[None, :, :, None]
    scores = (
        jnp.einsum("bthk,bshk->bhts", queries, key_raw, preferred_element_type=jnp.float32)
        * key_scale
    )
    grad_scores = jnp.einsum(
        "bthv,bshv->bhts", out_grad, values, preferred_element_type=jnp.float32
    )
    sums_ahead = jnp.einsum("bshk,bshv->bhkv", keys * keep_ahead, value_wide, precision=HIGHEST)
    sums_behind = jnp.einsum("bshk,bshv->bhkv", keys * keep_behind, value_wide, precision=HIGHEST)
    pulls_ahead = jnp.einsum(
        "bthk,bthv->bhkv", query_wide * reach_ahead, grad_wide, precision=HIGHEST
    )
    pulls_behind = jnp.einsum(
        "bthk,bthv->bhkv", query_wide * reach_behind, grad_wide, precision=HIGHEST
    )
    span_ahead = jnp.exp(length * rate_ahead).reshape(1, -1, 1, 1)
    span_behind = jnp.exp(length * rate_behind).reshape(1, -1, 1, 1)
    unit_span = jnp.ones_like(span_ahead)
    zero_state = jnp.zeros_like(sums_ahead)
    upward = prefix(
        (span_ahead, sums_ahead, span_behind, pulls_behind),
        "sp",
        link_states,
        (unit_span, zero_state, unit_span, zero_state),
        False,
    )
    downward = prefix(
        (span_behind, sums_behind, span_ahead, pulls_ahead),
        "sp",
        link_states,
        (unit_span, zero_state, unit_span, zero_state),
        True,
    )
    state_ahead, pull_behind = (upward[1], upward[3])
    state_behind, pull_ahead = (downward[1], downward[3])
    out_ahead = jnp.einsum(
        "bhts,bshv->bthv", scores * mask_ahead[None], value_wide, precision=HIGHEST
    )
    out_ahead = out_ahead + jnp.einsum(
        "bthk,bhkv->bthv", query_wide * reach_ahead, state_ahead, precision=HIGHEST
    )
    out_behind = jnp.einsum(
        "bhts,bshv->bthv", scores * mask_behind[None], value_wide, precision=HIGHEST
    )
    out_behind = out_behind + jnp.einsum(
        "bthk,bhkv->bthv", query_wide * reach_behind, state_behind, precision=HIGHEST
    )
    grad_q = jnp.einsum("bhts,bshk->bthk", grad_scores * mask_both, keys, precision=HIGHEST)
    grad_q = grad_q + reach_ahead * jnp.einsum(
        "bthv,bhkv->bthk", grad_wide, state_ahead, precision=HIGHEST
    )
    grad_q = grad_q + reach_behind * jnp.einsum(
        "bthv,bhkv->bthk", grad_wide, state_behind, precision=HIGHEST
    )
    grad_k_ahead = jnp.einsum(
        "bhts,bthk->bshk", grad_scores * mask_ahead[None], query_wide, precision=HIGHEST
    )
    grad_k_ahead = grad_k_ahead + keep_ahead * jnp.einsum(
        "bshv,bhkv->bshk", value_wide, pull_ahead, precision=HIGHEST
    )
    grad_k_behind = jnp.einsum(
        "bhts,bthk->bshk", grad_scores * mask_behind[None], query_wide, precision=HIGHEST
    )
    grad_k_behind = grad_k_behind + keep_behind * jnp.einsum(
        "bshv,bhkv->bshk", value_wide, pull_behind, precision=HIGHEST
    )
    grad_v = jnp.einsum("bhts,bthv->bshv", scores * mask_both, grad_wide, precision=HIGHEST)
    grad_v = grad_v + keep_ahead * jnp.einsum(
        "bshk,bhkv->bshv", keys, pull_ahead, precision=HIGHEST
    )
    grad_v = grad_v + keep_behind * jnp.einsum(
        "bshk,bhkv->bshv", keys, pull_behind, precision=HIGHEST
    )
    positions = (my_index * length + offsets)[None, :, None]
    out_dot_ahead = jnp.sum(positions * jnp.sum(out_ahead * grad_wide, axis=3), axis=(0, 1))
    key_dot_ahead = jnp.sum(positions * jnp.sum(keys * grad_k_ahead, axis=3), axis=(0, 1))
    out_dot_behind = jnp.sum(positions * jnp.sum(out_behind * grad_wide, axis=3), axis=(0, 1))
    key_dot_behind = jnp.sum(positions * jnp.sum(keys * grad_k_behind, axis=3), axis=(0, 1))
    local_sums = jnp.stack([out_dot_ahead - key_dot_ahead, key_dot_behind - out_dot_behind])
    rate_sums = lax.psum(local_sums, "sp")
    slopes = jnp.stack([jax.nn.sigmoid(-decay_ahead), jax.nn.sigmoid(-decay_behind)]) / all_tokens
    decay_grad = rate_sums * slopes
    key_grad_raw = ((grad_k_ahead + grad_k_behind) * key_scale).astype(jnp.bfloat16)

    def weight_rows(start, row_count):
        piece = lax.dynamic_slice_in_dim(inputs, start, row_count, 2)
        return jnp.einsum("bld,blhk->dhk", piece, key_grad_raw, preferred_element_type=jnp.float32)

    weight_grad = own_rows(weight_rows, in_width // devices, "sp")

    def input_rows(start, row_count):
        piece = lax.dynamic_slice_in_dim(key_grad_raw, start, row_count, 0)
        return jnp.einsum("blhk,dhk->bld", piece, key_weight, preferred_element_type=jnp.float32)

    input_grad = summed_rows(input_rows, batch_seqs // lax.axis_size("tp"), "tp").astype(
        jnp.bfloat16
    )
    return (
        grad_q.astype(jnp.bfloat16),
        grad_v.astype(jnp.bfloat16),
        input_grad,
        weight_grad,
        decay_grad,
    )


def solution(mesh):
    in_specs = (
        P(None, "sp", None),
        P(None, "sp", "tp", None),
        P(None, "sp", "tp", None),
        P(None, "sp", "tp", None),
        P(None, "tp", None),
        P("tp"),
        P("tp"),
    )
    out_specs = (
        P(None, "sp", "tp", None),
        P(None, "sp", "tp", None),
        P("tp", "sp", None),
        P("sp", "tp", None),
        P(None, "tp"),
    )
    return jax.shard_map(shards, mesh=mesh, in_specs=in_specs, out_specs=out_specs, check_vma=False)
```

profile of v0, /device:TPU:0, one launch (start us, length us, event | category | flops | bytes accessed | tf_op | source)
XLA Modules:
  0.0 462.7 jit_solution(7390019577858132643)
XLA Ops:
  10.9 2.1 fusion.41
  14.8 2.1 fusion.37
  17.1 2.1 fusion.40
  19.2 2.1 fusion.36
  23.7 36.6 %all-reduce.3 = (f32[32]{0:T(128)S(1)}, f32[32]{0:T(128)S(1)}) all-reduce(f32[32]{0:T(128)S(1)} %exponential_dynamic-update-slice_fusion, f32[32]{0:T(128)S(1)} %exponential_dynamic-update-slice_fusion.1), channel_id=4, replica_groups=mesh['sp'=16,'tp'=2] {'sp'}, use_global_device_ids=true, to_apply=%add.1 | all-reduce | flops 64 | bytes 512
  63.4 1.7 copy.122
  65.1 1.7 copy.144
  70.5 19.9 %all-gather.15.cloned.1.call-done = f32[32,2,128,256]{3,2,1,0:T(8,128)} async-done(((f32[2,2,128,256]{3,2,1,0:T(8,128)}), f32[32,2,128,256]{3,2,1,0:T(8,128)}) %all-gather.15.cloned.1.call-update) | async-done | bytes 8388624 | tf_op jit(solution)/shard_map/all_gather | solution.py:12
  90.5 7.6 %rev.13 = f32[16,2,2,128,256]{4,3,2,1,0:T(8,128)} reverse(f32[16,2,2,128,256]{4,3,2,1,0:T(8,128)} %bitcast.160), dimensions={0} | reverse | bytes 16777216 | tf_op jit(solution)/shard_map/rev | solution.py:14
  98.1 67.5 %all-gather.17.cloned.1.call-done = f32[32,2,128,256]{3,2,1,0:T(8,128)} async-done(((f32[2,2,128,256]{3,2,1,0:T(8,128)}), f32[32,2,128,256]{3,2,1,0:T(8,128)}) %all-gather.17.cloned.1.call-update) | async-done | bytes 8388624 | tf_op jit(solution)/shard_map/all_gather | solution.py:12
  165.6 7.6 %rev.15 = f32[16,2,2,128,256]{4,3,2,1,0:T(8,128)} reverse(f32[16,2,2,128,256]{4,3,2,1,0:T(8,128)} %bitcast.161), dimensions={0} | reverse | bytes 16777216 | tf_op jit(solution)/shard_map/rev | solution.py:14
  173.1 42.3 %while.33 = (s32[]{:T(128)}, f32[2,2,128,256]{3,2,1,0:T(8,128)S(1)}, f32[2,2,128,256]{3,2,1,0:T(8,128)S(1)}, s32[]{:T(128)}, f32[16,1,2,1,1]{2,4,3,1,0:T(1,128)}...) while((s32[]{:T(128)}, ...), condition=%wide.region_3.4_spmd.clone, body=%wide.region_2.3_spmd.clone.sunk | while | flops 1048580 | bytes 3145917 | solution.py:24
  199.5 1.8 fusion.118
  218.0 22.7 %all-gather.11.cloned.1.call-done = f32[32,2,128,256]{3,2,1,0:T(8,128)} async-done(((f32[2,2,128,256]{3,2,1,0:T(8,128)}), f32[32,2,128,256]{3,2,1,0:T(8,128)}) %all-gather.11.cloned.1.call-update) | async-done | bytes 8388624 | tf_op jit(solution)/shard_map/all_gather | solution.py:12
  240.6 74.9 %all-gather.13.cloned.1.call-done = f32[32,2,128,256]{3,2,1,0:T(8,128)} async-done(((f32[2,2,128,256]{3,2,1,0:T(8,128)}), f32[32,2,128,256]{3,2,1,0:T(8,128)}) %all-gather.13.cloned.1.call-update) | async-done | bytes 8388624 | tf_op jit(solution)/shard_map/all_gather | solution.py:12
  315.6 23.2 %while.32 = (s32[]{:T(128)}, f32[2,2,128,256]{3,2,1,0:T(8,128)S(1)}, f32[2,2,128,256]{3,2,1,0:T(8,128)S(1)}, s32[]{:T(128)}, f32[16,1,2,1,1]{2,4,3,1,0:T(1,128)S...) while((s32[]{:T(128)}, ...), condition=%wide.region_1.2_spmd.clone, body=%wide.region_0.1_spmd.clone.sunk | while | flops 1048580 | bytes 3145917 | solution.py:24
  341.3 1.8 fusion.38
  344.4 2.2 copy.136
  347.4 1.6 fusion.18
  351.7 31.6 %psum.7 = f32[2,2]{1,0:T(2,128)S(1)} all-reduce(f32[2,2]{1,0:T(2,128)S(1)} %pad_maximum_fusion), channel_id=1, replica_groups=mesh['sp'=16,'tp'=2] {'sp'}, use_global_device_ids=true, to_apply=%region_14.15 | all-reduce | flops 4 | bytes 32 | tf_op jit(solution)/shard_map/psum | solution.py:154
  383.3 1.7 fusion.28
  385.8 2.2 fusion.8
  392.8 46.6 %all-reduce.6.cloned.1.call-done = f32[1024,2,128]{2,1,0:T(2,128)} async-done(((f32[1024,2,128]{2,1,0:T(2,128)}), f32[1024,2,128]{2,1,0:T(2,128)}) %all-reduce.6.cloned.1.call-update) | async-done | bytes 1048592
  440.9 15.0 %reduce-scatter.2.cloned.1.call-done = bf16[1,128,1024]{2,1,0:T(8,128)(2,1)} async-done(((bf16[2,128,1024]{2,1,0:T(8,128)(2,1)}), bf16[1,128,1024]{2,1,0:T(8,128)(2,1)}) %reduce-scatter.2.cloned.1.call-update) | async-done | bytes 262160 | tf_op jit(solution)/shard_map/reduce_scatter | solution.py:34
  (177 shorter events, 92.8 us)
Async XLA Ops:
  7.2 2.8 copy-start
  7.2 62.4 %copy-start.2 = (bf16[2,128,2,256]{3,2,1,0:T(2,128)(2,1)S(1)}, bf16[2,128,2,256]{3,2,1,0:T(2,128)(2,1)}, u32[]{:S(2)}) copy-start(bf16[2,128,2,256]{3,2,1,0:T(2,128)(2,1)} %param.13) | copy-start | bytes 786436
  7.2 62.4 %copy-start.1 = (bf16[2,128,2,256]{3,2,1,0:T(2,128)(2,1)S(1)}, bf16[2,128,2,256]{3,2,1,0:T(2,128)(2,1)}, u32[]{:S(2)}) copy-start(bf16[2,128,2,256]{3,2,1,0:T(2,128)(2,1)} %param.14) | copy-start | bytes 786436
  7.2 83.3 %all-gather.15.cloned.1.call-start = ((), (), s32[]{:S(2)}) async-start(), calls=%async_computation.4 | async-start | bytes 8912896 | tf_op jit(solution)/shard_map/all_gather | solution.py:12
  9.9 11.6 %copy-start.12 = (f32[2]{0:T(128)}, f32[2]{0:T(128)S(1)}, u32[]{:S(2)}) copy-start(f32[2]{0:T(128)S(1)} %get-tuple-element.478) | copy-start | bytes 28
  9.9 11.6 %copy-start.13 = (f32[2]{0:T(128)}, f32[2]{0:T(128)S(1)}, u32[]{:S(2)}) copy-start(f32[2]{0:T(128)S(1)} %get-tuple-element.450) | copy-start | bytes 28
  10.9 10.5 %copy-start.8 = (f32[128,2]{0,1:T(2,128)}, f32[128,2]{0,1:T(2,128)S(1)}, u32[]{:S(2)}) copy-start(f32[128,2]{0,1:T(2,128)S(1)} %get-tuple-element.470) | copy-start | bytes 3076
  13.1 152.5 %all-gather.17.cloned.1.call-start = ((), (), s32[]{:S(2)}) async-start(), calls=%async_computation.5 | async-start | bytes 8912896 | tf_op jit(solution)/shard_map/all_gather | solution.py:12
  14.8 6.6 %copy-start.6 = (f32[128,2]{0,1:T(2,128)}, f32[128,2]{0,1:T(2,128)S(1)}, u32[]{:S(2)}) copy-start(f32[128,2]{0,1:T(2,128)S(1)} %get-tuple-element.467) | copy-start | bytes 3076
  17.0 223.6 %all-gather.11.cloned.1.call-start = ((), (), s32[]{:S(2)}) async-start(), calls=%async_computation.2 | async-start | bytes 8912896 | tf_op jit(solution)/shard_map/all_gather | solution.py:12
  19.2 296.4 %all-gather.13.cloned.1.call-start = ((), (), s32[]{:S(2)}) async-start(), calls=%async_computation.3 | async-start | bytes 8912896 | tf_op jit(solution)/shard_map/all_gather | solution.py:12
  21.4 418.0 %all-reduce.6.cloned.1.call-start = ((), (), s32[]{:S(2)}) async-start(), calls=%async_computation.6 | async-start | bytes 2097152
  173.1 42.3 %copy-start.9 = (f32[128,2]{0,1:T(2,128)S(1)}, f32[128,2]{0,1:T(2,128)}, u32[]{:S(2)}) copy-start(f32[128,2]{0,1:T(2,128)} %copy-done.8) | copy-start | bytes 3076
  315.6 25.4 %copy-start.3 = (f32[2,2,128,128]{3,2,1,0:T(8,128)S(1)}, f32[2,2,128,128]{3,2,1,0:T(8,128)}, u32[]{:S(2)}) copy-start(f32[2,2,128,128]{3,2,1,0:T(8,128)} %fusion.72) | copy-start | bytes 786436
  315.6 25.4 %copy-start.5 = (f32[2,128,128]{2,1,0:T(8,128)S(1)}, f32[2,128,128]{2,1,0:T(8,128)}, u32[]{:S(2)}) copy-start(f32[2,128,128]{2,1,0:T(8,128)} %get-tuple-element.459) | copy-start | bytes 393220
  338.7 8.0 %copy-start.7 = (f32[128,2]{0,1:T(2,128)S(1)}, f32[128,2]{0,1:T(2,128)}, u32[]{:S(2)}) copy-start(f32[128,2]{0,1:T(2,128)} %copy-done.6) | copy-start | bytes 3076
  338.8 8.6 %copy-start.4 = (f32[2,2,128,128]{2,3,1,0:T(8,128)S(1)}, f32[2,2,128,128]{2,3,1,0:T(8,128)}, u32[]{:S(2)}) copy-start(f32[2,2,128,128]{2,3,1,0:T(8,128)} %convolution_bitcast_fusion.16) | copy-start | bytes 786436
  339.9 48.1 %copy-start.10 = (f32[128,2]{0,1:T(2,128)S(1)}, f32[128,2]{0,1:T(2,128)}, u32[]{:S(2)}) copy-start(f32[128,2]{0,1:T(2,128)} %get-tuple-element.468) | copy-start | bytes 3076
  340.9 47.7 %copy-start.11 = (f32[128,2]{0,1:T(2,128)S(1)}, f32[128,2]{0,1:T(2,128)}, u32[]{:S(2)}) copy-start(f32[128,2]{0,1:T(2,128)} %get-tuple-element.461) | copy-start | bytes 3076
  346.7 109.2 %reduce-scatter.2.cloned.1.call-start = ((), (), s32[]{:S(2)}) async-start(), calls=%async_computation.1 | async-start | bytes 786432 | tf_op jit(solution)/shard_map/reduce_scatter | solution.py:34
Sparse Core Ops, SparseCore 0:
  13.2 77.2 all-gather.14
  92.6 72.8 all-gather.16
  167.7 72.8 all-gather.10
  242.6 72.8 all-gather.12
  346.8 92.5 all-reduce.5
  442.1 13.7 reduce-scatter.1
where the time goes:
time: 464 us; the launch traced here: 463 us
  waiting for transfers between devices  247 us (53%)
  blocking collectives  68.2 us (15%)
  other arithmetic  51.9 us (11%)
  local copies, waits for them, and re-layouts  49.5 us (11%)
  matrix products  29.3 us (6%)
  between operations  15.8 us (3%)
    all_gather x4, waiting for transfers between devices, prefix(): pieces = jax.tree.map(lambda part: lax.all_gather(part, axis), value)  185 us
    unnamed x7, waiting for transfers between devices  46.7 us
    select_n x30, other arithmetic, step(): jnp.where(position < mine, new, old)  44.9 us
    unnamed x1, blocking collectives  36.6 us
    psum x1, blocking collectives, shards(): rate_sums = lax.psum(local_sums, 'sp')  31.6 us
    rev x4, local copies, waits for them, and re-layouts, prefix(): pieces = jax.tree.map(lambda part: part[::-1], pieces)  16.4 us
    reduce_scatter x1, waiting for transfers between devices, summed_rows(): lax.psum_scatter(everything.astype(jnp.bfloat16), axis, scatter_dimension...  15 us
    mul x30, local copies, waits for them, and re-layouts, link_states(): later[0] * earlier[1] + later[1]  9.94 us
  transfers between devices with their start and end apart: 6, of which 6 were waited for; matrix products, arithmetic and copies ran while one was open for 20% of the time, Pallas kernels for 0%

commit v1 on v0

--- a/solution.py
+++ b/solution.py
@@ -151,7 +151,7 @@
     out_dot_behind = jnp.sum(positions * jnp.sum(out_behind * grad_wide, axis=3), axis=(0, 1))
     key_dot_behind = jnp.sum(positions * jnp.sum(keys * grad_k_behind, axis=3), axis=(0, 1))
     local_sums = jnp.stack([out_dot_ahead - key_dot_ahead, key_dot_behind - out_dot_behind])
-    rate_sums = lax.psum(local_sums, "sp")
+    rate_sums = jnp.sum(lax.all_gather(local_sums, "sp"), axis=0)
     slopes = jnp.stack([jax.nn.sigmoid(-decay_ahead), jax.nn.sigmoid(-decay_behind)]) / all_tokens
     decay_grad = rate_sums * slopes
     key_grad_raw = ((grad_k_ahead + grad_k_behind) * key_scale).astype(jnp.bfloat16)

time: 464 us -> 494 us (1.065)
  waiting for transfers between devices: 247 us -> 278 us
  blocking collectives: 68.2 us -> 55.7 us
  local copies, waits for them, and re-layouts: 49.5 us -> 58.3 us
    psum x1 -> x0, blocking collectives: 31.6 us -> none  [shards(): rate_sums = lax.psum(local_sums, 'sp')]
    all_gather x0 -> x1, blocking collectives: none -> 19.1 us  [shards(): rate_sums = jnp.sum(lax.all_gather(local_sums, 'sp'), axis=0)]
    all_gather x4, waiting for transfers between devices: 185 us -> 202 us  [prefix(): pieces = jax.tree.map(lambda part: lax.all_gather(part, axis), value)]
    unnamed x7, waiting for transfers between devices: 46.7 us -> 60.7 us
    mul x30, local copies, waits for them, and re-layouts: 9.63 us -> 17.5 us  [link_states(): later[2] * earlier[3] + later[3]]
  transfers between devices with their start and end apart: 6 -> 6, of which waited for: 6 -> 6; matrix products, arithmetic and copies ran while one was open for 20% -> 15% of each run, Pallas kernels for 0% -> 0%
where the time goes in v1:
time: 494 us; the launch traced here: 492 us
  waiting for transfers between devices  278 us (56%)
  local copies, waits for them, and re-layouts  58.3 us (12%)
  blocking collectives  55.7 us (11%)
  other arithmetic  51.8 us (10%)
  matrix products  32.2 us (7%)
  between operations  15.8 us (3%)
    all_gather x4, waiting for transfers between devices, prefix(): pieces = jax.tree.map(lambda part: lax.all_gather(part, axis), value)  202 us
    unnamed x7, waiting for transfers between devices  60.7 us
    select_n x30, other arithmetic, step(): jnp.where(position < mine, new, old)  44.6 us
    unnamed x1, blocking collectives  36.6 us
    all_gather x1, blocking collectives, shards(): rate_sums = jnp.sum(lax.all_gather(local_sums, 'sp'), axis=0)  19.1 us
    mul x30, local copies, waits for them, and re-layouts, link_states(): later[2] * earlier[3] + later[3]  17.5 us
    rev x4, local copies, waits for them, and re-layouts, prefix(): pieces = jax.tree.map(lambda part: part[::-1], pieces)  16.4 us
    reduce_scatter x1, waiting for transfers between devices, summed_rows(): lax.psum_scatter(everything.astype(jnp.bfloat16), axis, scatter_dimension...  15 us
  transfers between devices with their start and end apart: 6, of which 6 were waited for; matrix products, arithmetic and copies ran while one was open for 15% of the time, Pallas kernels for 0%

profile of v1, /device:TPU:0, one launch (start us, length us, event | category | flops | bytes accessed | tf_op | source)
XLA Modules:
  0.0 492.3 jit_solution(453573500507484473)
XLA Ops:
  10.9 2.1 fusion.41
  13.8 2.1 fusion.40
  17.0 2.1 fusion.36
  19.2 2.1 fusion.37
  23.8 36.6 %all-reduce.3 = (f32[32]{0:T(128)S(1)}, f32[32]{0:T(128)S(1)}) all-reduce(f32[32]{0:T(128)S(1)} %exponential_dynamic-update-slice_fusion, f32[32]{0:T(128)S(1)} %exponential_dynamic-update-slice_fusion.1), channel_id=4, replica_groups=mesh['sp'=16,'tp'=2] {'sp'}, use_global_device_ids=true, to_apply=%add.1 | all-reduce | flops 64 | bytes 512
  63.4 1.7 copy.122
  65.1 1.7 copy.144
  66.8 1.6 copy.137
  71.6 18.9 %all-gather.17.cloned.1.call-done = f32[32,2,128,256]{3,2,1,0:T(8,128)} async-done(((f32[2,2,128,256]{3,2,1,0:T(8,128)}), f32[32,2,128,256]{3,2,1,0:T(8,128)}) %all-gather.17.cloned.1.call-update) | async-done | bytes 8388624 | tf_op jit(solution)/shard_map/all_gather | solution.py:12
  90.5 7.6 %rev.13 = f32[16,2,2,128,256]{4,3,2,1,0:T(8,128)} reverse(f32[16,2,2,128,256]{4,3,2,1,0:T(8,128)} %bitcast.163), dimensions={0} | reverse | bytes 16777216 | tf_op jit(solution)/shard_map/rev | solution.py:14
  98.1 67.5 %all-gather.13.cloned.1.call-done = f32[32,2,128,256]{3,2,1,0:T(8,128)} async-done(((f32[2,2,128,256]{3,2,1,0:T(8,128)}), f32[32,2,128,256]{3,2,1,0:T(8,128)}) %all-gather.13.cloned.1.call-update) | async-done | bytes 8388624 | tf_op jit(solution)/shard_map/all_gather | solution.py:12
  165.6 75.1 %all-gather.15.cloned.1.call-done = f32[32,2,128,256]{3,2,1,0:T(8,128)} async-done(((f32[2,2,128,256]{3,2,1,0:T(8,128)}), f32[32,2,128,256]{3,2,1,0:T(8,128)}) %all-gather.15.cloned.1.call-update) | async-done | bytes 8388624 | tf_op jit(solution)/shard_map/all_gather | solution.py:12
  240.6 30.6 %while.32 = (s32[]{:T(128)}, f32[2,2,128,256]{3,2,1,0:T(8,128)S(1)}, f32[2,2,128,256]{3,2,1,0:T(8,128)S(1)}, s32[]{:T(128)}, f32[16,1,2,1,1]{2,4,3,1,0:T(1,128)S...) while((s32[]{:T(128)}, ...), condition=%wide.region_1.2_spmd.clone, body=%wide.region_0.1_spmd.clone.sunk | while | flops 1048580 | bytes 3145917 | solution.py:24
  271.2 1.8 fusion.20
  273.0 2.1 fusion.16
  275.2 40.4 %all-gather.19.cloned.1.call-done = f32[32,2,128,256]{3,2,1,0:T(8,128)} async-done(((f32[2,2,128,256]{3,2,1,0:T(8,128)}), f32[32,2,128,256]{3,2,1,0:T(8,128)}) %all-gather.19.cloned.1.call-update) | async-done | bytes 8388624 | tf_op jit(solution)/shard_map/all_gather | solution.py:12
  315.6 7.6 %rev.15 = f32[16,2,2,128,256]{4,3,2,1,0:T(8,128)} reverse(f32[16,2,2,128,256]{4,3,2,1,0:T(8,128)} %bitcast.162), dimensions={0} | reverse | bytes 16777216 | tf_op jit(solution)/shard_map/rev | solution.py:14
  323.2 42.1 %while.33 = (s32[]{:T(128)}, f32[2,2,128,256]{3,2,1,0:T(8,128)S(1)}, f32[2,2,128,256]{3,2,1,0:T(8,128)S(1)}, s32[]{:T(128)}, f32[16,1,2,1,1]{2,4,3,1,0:T(1,128)}...) while((s32[]{:T(128)}, ...), condition=%wide.region_3.4_spmd.clone, body=%wide.region_2.3_spmd.clone.sunk | while | flops 1048580 | bytes 3145917 | solution.py:24
  369.7 2.2 fusion.8
  374.3 2.2 copy.136
  379.2 1.7 fusion.28
  388.0 19.1 %all-gather.7 = f32[16,2,2]{2,1,0:T(2,128)S(1)} all-gather(f32[1,2,2]{2,1,0:T(2,128)S(1)} %maximum_bitcast_fusion), channel_id=8, replica_groups=mesh['sp'=16,'tp'=2] {'sp'}, dimensions={0}, use_global_device_ids=true | all-gather | bytes 272 | tf_op jit(solution)/shard_map/all_gather | solution.py:154
  408.4 60.6 %all-reduce.6.cloned.1.call-done = f32[1024,2,128]{2,1,0:T(2,128)} async-done(((f32[1024,2,128]{2,1,0:T(2,128)}), f32[1024,2,128]{2,1,0:T(2,128)}) %all-reduce.6.cloned.1.call-update) | async-done | bytes 1048592
  470.5 15.0 %reduce-scatter.2.cloned.1.call-done = bf16[1,128,1024]{2,1,0:T(8,128)(2,1)} async-done(((bf16[2,128,1024]{2,1,0:T(8,128)(2,1)}), bf16[1,128,1024]{2,1,0:T(8,128)(2,1)}) %reduce-scatter.2.cloned.1.call-update) | async-done | bytes 262160 | tf_op jit(solution)/shard_map/reduce_scatter | solution.py:34
  (174 shorter events, 104.0 us)
Async XLA Ops:
  7.2 2.8 copy-start
  7.2 63.5 %copy-start.2 = (bf16[2,128,2,256]{3,2,1,0:T(2,128)(2,1)S(1)}, bf16[2,128,2,256]{3,2,1,0:T(2,128)(2,1)}, u32[]{:S(2)}) copy-start(bf16[2,128,2,256]{3,2,1,0:T(2,128)(2,1)} %param.13) | copy-start | bytes 786436
  7.2 63.5 %copy-start.1 = (bf16[2,128,2,256]{3,2,1,0:T(2,128)(2,1)S(1)}, bf16[2,128,2,256]{3,2,1,0:T(2,128)(2,1)}, u32[]{:S(2)}) copy-start(bf16[2,128,2,256]{3,2,1,0:T(2,128)(2,1)} %param.14) | copy-start | bytes 786436
  7.2 83.3 %all-gather.17.cloned.1.call-start = ((), (), s32[]{:S(2)}) async-start(), calls=%async_computation.4 | async-start | bytes 8912896 | tf_op jit(solution)/shard_map/all_gather | solution.py:12
  9.9 11.6 %copy-start.10 = (f32[2]{0:T(128)}, f32[2]{0:T(128)S(1)}, u32[]{:S(2)}) copy-start(f32[2]{0:T(128)S(1)} %get-tuple-element.478) | copy-start | bytes 28
  9.9 11.6 %copy-start.11 = (f32[2]{0:T(128)}, f32[2]{0:T(128)S(1)}, u32[]{:S(2)}) copy-start(f32[2]{0:T(128)S(1)} %get-tuple-element.450) | copy-start | bytes 28
  10.9 10.5 %copy-start.5 = (f32[128,2]{0,1:T(2,128)}, f32[128,2]{0,1:T(2,128)S(1)}, u32[]{:S(2)}) copy-start(f32[128,2]{0,1:T(2,128)S(1)} %get-tuple-element.470) | copy-start | bytes 3076
  13.1 152.5 %all-gather.13.cloned.1.call-start = ((), (), s32[]{:S(2)}) async-start(), calls=%async_computation.2 | async-start | bytes 8912896 | tf_op jit(solution)/shard_map/all_gather | solution.py:12
  13.8 7.6 %copy-start.7 = (f32[128,2]{0,1:T(2,128)}, f32[128,2]{0,1:T(2,128)S(1)}, u32[]{:S(2)}) copy-start(f32[128,2]{0,1:T(2,128)S(1)} %get-tuple-element.467) | copy-start | bytes 3076
  15.9 224.7 %all-gather.15.cloned.1.call-start = ((), (), s32[]{:S(2)}) async-start(), calls=%async_computation.3 | async-start | bytes 8912896 | tf_op jit(solution)/shard_map/all_gather | solution.py:12
  19.2 296.4 %all-gather.19.cloned.1.call-start = ((), (), s32[]{:S(2)}) async-start(), calls=%async_computation.5 | async-start | bytes 8912896 | tf_op jit(solution)/shard_map/all_gather | solution.py:12
  21.4 447.6 %all-reduce.6.cloned.1.call-start = ((), (), s32[]{:S(2)}) async-start(), calls=%async_computation.6 | async-start | bytes 2097152
  323.2 42.1 %copy-start.9 = (f32[128,2]{0,1:T(2,128)S(1)}, f32[128,2]{0,1:T(2,128)}, u32[]{:S(2)}) copy-start(f32[128,2]{0,1:T(2,128)} %get-tuple-element.461) | copy-start | bytes 3076
  323.2 43.9 %copy-start.3 = (f32[2,2,128,128]{3,2,1,0:T(8,128)S(1)}, f32[2,2,128,128]{3,2,1,0:T(8,128)}, u32[]{:S(2)}) copy-start(f32[2,2,128,128]{3,2,1,0:T(8,128)} %fusion.72) | copy-start | bytes 786436
  323.2 50.0 %copy-start.6 = (f32[128,2]{0,1:T(2,128)S(1)}, f32[128,2]{0,1:T(2,128)}, u32[]{:S(2)}) copy-start(f32[128,2]{0,1:T(2,128)} %copy-done.5) | copy-start | bytes 3076
  365.2 11.5 %copy-start.8 = (f32[128,2]{0,1:T(2,128)S(1)}, f32[128,2]{0,1:T(2,128)}, u32[]{:S(2)}) copy-start(f32[128,2]{0,1:T(2,128)} %copy-done.7) | copy-start | bytes 3076
  365.3 15.6 %copy-start.4 = (f32[2,2,128,128]{2,3,1,0:T(8,128)S(1)}, f32[2,2,128,128]{2,3,1,0:T(8,128)}, u32[]{:S(2)}) copy-start(f32[2,2,128,128]{2,3,1,0:T(8,128)} %convolution_bitcast_fusion.16) | copy-start | bytes 786436
  376.5 108.9 %reduce-scatter.2.cloned.1.call-start = ((), (), s32[]{:S(2)}) async-start(), calls=%async_computation.1 | async-start | bytes 786432 | tf_op jit(solution)/shard_map/reduce_scatter | solution.py:34
Sparse Core Ops, SparseCore 0:
  13.2 77.2 all-gather.16
  92.6 72.8 all-gather.12
  167.7 72.8 all-gather.14
  242.6 72.8 all-gather.18
  376.7 92.3 all-reduce.5
  471.7 13.7 reduce-scatter.1
